TPU v7x, 32 devices: a whole 2x2x4 slice. The times are simulated.
32 devices in a mesh: sp: 8 (over z, y), tp: 4 (over x, core).
Axes of the slice: x: 2, y: 2, z: 4, core: 2. Of those that a mesh axis runs over, the one named last changes fastest.
Arguments:
- residual: bfloat16 [8192, 2048], P(('sp', 'tp')), may hold values from -6 to 6
- first_group_queries: bfloat16 [8192, 1024], P('sp', 'tp'), may hold values from -6 to 6
- first_group_keys: bfloat16 [8192, 1024], P('sp', 'tp'), may hold values from -6 to 6
- second_group_queries: bfloat16 [8192, 512], P('sp', 'tp'), may hold values from -6 to 6
- second_group_keys: bfloat16 [8192, 512], P('sp', 'tp'), may hold values from -6 to 6
- primary_retain_switch_inputs: bfloat16 [8192, 1024], P('sp', 'tp'), may hold values from -12 to 16
- secondary_retain_switch_inputs: bfloat16 [8192, 512], P('sp', 'tp'), may hold values from -12 to 16
- timestep_fading_exponent: float32 [8192], P('sp'), may hold values from -2.1 to 0
- values: bfloat16 [2, 8192, 1024], P(None, 'sp', 'tp'), may hold values from -6 to 6
- output_gate_logits: bfloat16 [2, 8192, 1024], P(None, 'sp', 'tp'), may hold values from -6 to 6
- head_norm_gains: float32 [2, 1024], P(None, 'tp'), may hold values from 0.1 to 1.9
- output_projection: bfloat16 [2, 1024, 2048], P(None, 'tp'), may hold values from -0.125 to 0.125
- feedforward_norm_gain: float32 [2048], replicated, may hold values from 0.1 to 1.9
- gate_projection: bfloat16 [2048, 6144], P('sp', 'tp'), may hold values from -0.125 to 0.125
- up_projection: bfloat16 [2048, 6144], P('sp', 'tp'), may hold values from -0.125 to 0.125
- down_projection: bfloat16 [6144, 2048], P('tp', 'sp'), may hold values from -0.078125 to 0.078125
Outputs:
- layer_out: bfloat16 [8192, 2048], P(('sp', 'tp'))
All inputs are finite; a program needn't handle non-finite values.
Results may differ from a plain program's by a relative error of at most 0.018.
Values may be sent and summed in bfloat16 or wider, within the bound.
A program may use at most 128 MiB of HBM per device.

v0:
```python
import jax
import jax.numpy as jnp
from jax import lax
from jax.sharding import PartitionSpec as P

FIRST_KEY_SIZE = 128
SECOND_KEY_SIZE = 64
DV = 128
BLOCK = 64


EPS = 1e-06
SOFTNESS_SCALE = 16.0
highest_precision = lax.Precision.HIGHEST


def entering(shard, axis, combine, identity):
    peers, place = (lax.axis_size(axis), lax.axis_index(axis))
    everything = jax.tree.map(
        lambda part, kind: lax.all_gather(part.astype(kind), axis),
        shard,
        (jnp.bfloat16, jnp.bfloat16, jnp.bfloat16, jnp.bfloat16),
    )
    start = jax.tree.map(
        lambda part, zero: jnp.broadcast_to(jnp.asarray(zero, part.dtype), part.shape),
        shard,
        identity,
    )

    def step(k, before):
        reached = k < place
        new = combine(
            before, jax.tree.map(lambda part, own: part[k].astype(own.dtype), everything, shard)
        )
        return jax.tree.map(lambda a, b: jnp.where(reached, a, b), new, before)

    return lax.fori_loop(0, peers, step, start)


def blocks(source, block_count, head_count, key_width):
    return (
        source.astype(jnp.float32)
        .reshape(block_count, BLOCK, head_count, key_width)
        .transpose(0, 2, 1, 3)
    )


def within_block_pass(
    query_matrix_rows,
    key_matrix_rows,
    value_matrix_rows,
    retain_switch_lines,
    position_decay_rows,
    key_width,
):
    head_count = query_matrix_rows.shape[1] // key_width
    block_count = query_matrix_rows.shape[0] // BLOCK
    decay_logarithm = (
        jax.nn.log_sigmoid(retain_switch_lines.astype(jnp.float32)) / SOFTNESS_SCALE
        + position_decay_rows[:, None]
    )
    query_blocks = blocks(query_matrix_rows, block_count, head_count, key_width) * key_width ** (
        -0.5
    )
    key_blocks = blocks(key_matrix_rows, block_count, head_count, key_width)
    value_blocks = blocks(value_matrix_rows, block_count, head_count, DV)
    decay_blocks = jnp.cumsum(blocks(decay_logarithm, block_count, head_count, key_width), axis=2)
    causal = jnp.tril(jnp.ones((BLOCK, BLOCK), dtype=bool))

    def advance(running_state, inputs):
        query_piece, key_piece, value_piece, decay_piece = inputs
        spread_log = decay_piece[:, :, None, :] - decay_piece[:, None, :, :]
        decay_grid = jnp.exp(jnp.where(causal[None, :, :, None], spread_log, -jnp.inf))
        scores = jnp.sum(
            query_piece[:, :, None, :] * key_piece[:, None, :, :] * decay_grid, axis=-1
        )
        block_result = jnp.einsum("hij,hjv->hiv", scores, value_piece, precision=highest_precision)
        block_result = block_result + jnp.einsum(
            "rus,rsp->rup",
            query_piece * jnp.exp(decay_piece),
            running_state,
            precision=highest_precision,
        )
        final_log_decay = decay_piece[:, -1:, :]
        running_state = jnp.exp(final_log_decay[:, 0, :])[:, :, None] * running_state + jnp.einsum(
            "qxe,qxt->qet",
            key_piece * jnp.exp(final_log_decay - decay_piece),
            value_piece,
            precision=highest_precision,
        )
        return (running_state, block_result)

    zero_state = jnp.zeros((head_count, key_width, DV), jnp.float32)
    local_state, local_out = lax.scan(
        advance, zero_state, (query_blocks, key_blocks, value_blocks, decay_blocks)
    )
    block_totals = decay_blocks[:, :, -1, :]
    before_log = jnp.cumsum(block_totals, axis=0) - block_totals
    cross_block_term = query_blocks * jnp.exp(decay_blocks + before_log[:, :, None, :])
    decay_total = jnp.exp(jnp.sum(block_totals, axis=0))
    return (local_out, cross_block_term, decay_total, local_state)


def finish(local_out, cross_block_term, incoming_state, gate_rows, gain_row):
    carried_over = jnp.einsum(
        "pjli,jie->pjle", cross_block_term, incoming_state, precision=highest_precision
    )
    summed = (local_out + carried_over).transpose(0, 2, 1, 3)
    row_count = summed.shape[0] * summed.shape[1]
    summed = summed.reshape(row_count, summed.shape[2], summed.shape[3])
    inverse = lax.rsqrt(jnp.mean(summed * summed, axis=-1, keepdims=True) + EPS)
    normed = (summed * inverse).reshape(row_count, -1) * gain_row
    return (jax.nn.silu(gate_rows.astype(jnp.float32)) * normed).astype(jnp.bfloat16)


def join_states(earlier, after_part):
    return (
        earlier[0] * after_part[0],
        after_part[0][:, :, None] * earlier[1] + after_part[1],
        earlier[2] * after_part[2],
        after_part[2][:, :, None] * earlier[3] + after_part[3],
    )


def row_norm(source, gain_row):
    widened = source.astype(jnp.float32)
    inverse = lax.rsqrt(jnp.mean(widened * widened, axis=-1, keepdims=True) + EPS)
    return (widened * inverse * gain_row).astype(jnp.bfloat16)


def per_device(
    residual,
    first_group_queries,
    first_group_keys,
    second_group_queries,
    second_group_keys,
    primary_retain_switch_inputs,
    secondary_retain_switch_inputs,
    timestep_fading_exponent,
    values,
    output_gate_logits,
    head_norm_gains,
    output_projection,
    feedforward_norm_gain,
    gate_projection,
    up_projection,
    down_projection,
):
    out_a, reach_a, decay_a, state_a = within_block_pass(
        first_group_queries,
        first_group_keys,
        values[0],
        primary_retain_switch_inputs,
        timestep_fading_exponent,
        FIRST_KEY_SIZE,
    )
    out_b, reach_b, decay_b, state_b = within_block_pass(
        second_group_queries,
        second_group_keys,
        values[1],
        secondary_retain_switch_inputs,
        timestep_fading_exponent,
        SECOND_KEY_SIZE,
    )
    identity = (
        jnp.ones_like(decay_a),
        jnp.zeros_like(state_a),
        jnp.ones_like(decay_b),
        jnp.zeros_like(state_b),
    )
    incoming_state = entering((decay_a, state_a, decay_b, state_b), "sp", join_states, identity)
    gated_a = finish(out_a, reach_a, incoming_state[1], output_gate_logits[0], head_norm_gains[0])
    gated_b = finish(out_b, reach_b, incoming_state[3], output_gate_logits[1], head_norm_gains[1])
    attention = lax.psum_scatter(
        (
            jnp.dot(gated_a, output_projection[0], preferred_element_type=jnp.float32)
            + jnp.dot(gated_b, output_projection[1], preferred_element_type=jnp.float32)
        ).astype(jnp.bfloat16),
        "tp",
        scatter_dimension=0,
        tiled=True,
    ).astype(jnp.float32)
    mid_rows = (residual.astype(jnp.float32) + attention).astype(jnp.bfloat16)
    all_rows = lax.all_gather(row_norm(mid_rows, feedforward_norm_gain), "tp", axis=0, tiled=True)
    gate_sum = jnp.dot(
        all_rows,
        lax.all_gather(gate_projection, "sp", axis=0, tiled=True),
        preferred_element_type=jnp.float32,
    )
    up_sum = jnp.dot(
        all_rows,
        lax.all_gather(up_projection, "sp", axis=0, tiled=True),
        preferred_element_type=jnp.float32,
    )
    hidden = (jax.nn.silu(gate_sum) * up_sum).astype(jnp.bfloat16)
    down_terms = jnp.dot(
        hidden,
        lax.all_gather(down_projection, "sp", axis=1, tiled=True),
        preferred_element_type=jnp.float32,
    )
    down_sum = lax.psum_scatter(
        down_terms.astype(jnp.bfloat16), "tp", scatter_dimension=0, tiled=True
    ).astype(jnp.float32)
    return (mid_rows.astype(jnp.float32) + down_sum).astype(jnp.bfloat16)


def solution(mesh):
    return jax.shard_map(
        per_device,
        mesh=mesh,
        in_specs=(
            P(("sp", "tp"), None),
            P("sp", "tp"),
            P("sp", "tp"),
            P("sp", "tp"),
            P("sp", "tp"),
            P("sp", "tp"),
            P("sp", "tp"),
            P("sp"),
            P(None, "sp", "tp"),
            P(None, "sp", "tp"),
            P(None, "tp"),
            P(None, "tp", None),
            P(),
            P("sp", "tp"),
            P("sp", "tp"),
            P("tp", "sp"),
        ),
        out_specs=P(("sp", "tp"), None),
        check_vma=False,
    )
```

profile of v0, /device:TPU:0, one launch (start us, length us, event | category | flops | bytes accessed | tf_op | source)
XLA Modules:
  0.0 824.7 jit_solution(4554943083443910818)
XLA Ops:
  11.1 22.9 %all-gather.4 = bf16[8,2,128]{2,1,0:T(2,128)(2,1)} all-gather(bf16[1,2,128]{2,1,0:T(2,128)(2,1)S(1)} %fusion.86), channel_id=2, replica_groups=mesh['sp'=8,'tp'=4] {'sp'}, dimensions={0}, use_global_device_ids=true | all-gather | bytes 4608 | tf_op jit(solution)/shard_map/all_gather | solution.py:20
  37.3 16.9 %all-gather.5 = bf16[8,2,64]{2,1,0:T(2,128)(2,1)} all-gather(bf16[1,2,64]{2,1,0:T(2,128)(2,1)S(1)} %fusion.87), channel_id=4, replica_groups=mesh['sp'=8,'tp'=4] {'sp'}, dimensions={0}, use_global_device_ids=true | all-gather | bytes 2304 | tf_op jit(solution)/shard_map/all_gather | solution.py:20
  67.2 98.9 %while.42 = (s32[]{:T(128)}, f32[2,128,128]{2,1,0:T(8,128)S(1)}, f32[16,2,64,128]{3,2,0,1:T(8,128)}, f32[16,2,64,128]{3,0,1,2:T(8,128)S(1)}, f32[16,2,64,128]{3,...) while((s32[]{:T(128)}, f32[2,128,128]{2,1,0:T(8,128)S(1)}, ...), condition=%wide.region_3.4_spmd.clone, body=%wide.region_1.3_spmd.clone.sunk | while | flops 68349952 | bytes 2047092 | solution.py:94
  166.2 33.4 %all-gather.1 = bf16[16,128,128]{2,1,0:T(8,128)(2,1)} all-gather(bf16[2,128,128]{2,1,0:T(8,128)(2,1)S(1)} %convert_element_type.162), channel_id=3, replica_groups=mesh['sp'=8,'tp'=4] {'sp'}, dimensions={0}, use_global_device_ids=true | all-gather | bytes 589824 | tf_op jit(solution)/shard_map/all_gather | solution.py:20
  199.6 2.8 reshape.267
  209.1 105.1 %while.43 = (s32[]{:T(128)}, f32[2,64,128]{2,1,0:T(8,128)S(1)}, f32[16,2,64,128]{3,2,0,1:T(8,128)}, f32[16,2,64,64]{3,0,1,2:T(8,128)}, f32[16,2,64,64]{3,1,2,0:T...) while((s32[]{:T(128)}, f32[2,64,128]{2,1,0:T(8,128)S(1)}, ...), condition=%wide.region_9.10_spmd.clone, body=%wide.region_7.9_spmd.clone.sunk | while | flops 40472576 | bytes 1420916 | solution.py:94
  314.2 30.9 %all-gather.3 = bf16[16,64,128]{2,1,0:T(8,128)(2,1)S(1)} all-gather(bf16[2,64,128]{2,1,0:T(8,128)(2,1)S(1)} %convert_element_type.168), channel_id=5, replica_groups=mesh['sp'=8,'tp'=4] {'sp'}, dimensions={0}, use_global_device_ids=true | all-gather | bytes 294912 | tf_op jit(solution)/shard_map/all_gather | solution.py:20
  345.2 35.0 %while.44 = (s32[]{:T(128)}, f32[2,128,128]{2,1,0:T(8,128)}, f32[2,64,128]{2,1,0:T(8,128)}, s32[]{:T(128)}, bf16[8,2,128]{2,1,0:T(2,128)(2,1)}, /*index=5*/bf16[...) while((s32[]{:T(128)}, f32[2,128,128]{2,1,0:T(8,128)}, ...), condition=%wide.region_11.12_spmd.clone, body=%wide.region_10.11_spmd.clone.sunk | while | flops 246148 | bytes 495499 | solution.py:37
  381.5 3.0 multiply_reduce_fusion.3
  394.7 3.0 multiply_reduce_fusion.2
  398.8 3.0 mul.280
  401.8 3.1 mul.281
  406.7 3.0 reshape.259
  409.7 2.9 fusion.53
  412.6 3.6 add_convert_fusion
  416.9 43.0 %reduce-scatter.3.cloned.1.call-done = bf16[256,2048]{1,0:T(8,128)(2,1)} async-done(((bf16[1024,2048]{1,0:T(8,128)(2,1)}), bf16[256,2048]{1,0:T(8,128)(2,1)}) %reduce-scatter.3.cloned.1.call-update) | async-done | bytes 1048592 | tf_op jit(solution)/shard_map/reduce_scatter | solution.py:174
  465.8 50.6 %all-gather.13.cloned.1.call-done = bf16[2048,1536]{1,0:T(8,128)(2,1)} async-done(((bf16[256,1536]{1,0:T(8,128)(2,1)}), bf16[2048,1536]{1,0:T(8,128)(2,1)}) %all-gather.13.cloned.1.call-update) | async-done | bytes 6291472 | tf_op jit(solution)/shard_map/all_gather | solution.py:187
  516.3 34.0 %all-gather.11.cloned.1.call-done = bf16[1024,2048]{1,0:T(8,128)(2,1)} async-done(((bf16[256,2048]{1,0:T(8,128)(2,1)}), bf16[1024,2048]{1,0:T(8,128)(2,1)}) %all-gather.11.cloned.1.call-update) | async-done | bytes 4194320 | tf_op jit(solution)/shard_map/all_gather | solution.py:184
  550.3 11.7 %fusion.91 = f32[1024,1536]{1,0:T(8,128)} fusion(bf16[1024,2048]{1,0:T(8,128)(2,1)} %all-gather.11.cloned.1.call-done, bf16[2048,1536]{1,0:T(8,128)(2,1)} %all-gather.13.cloned.1.call-done), kind=kOutput, calls=%fused_computation.148 | convolution fusion | flops 6442450944 | bytes 16777216 | tf_op jit(solution)/shard_map/dot_general | solution.py:185
  562.0 88.9 %all-gather.15.cloned.1.call-done = bf16[2048,1536]{1,0:T(8,128)(2,1)} async-done(((bf16[256,1536]{1,0:T(8,128)(2,1)}), bf16[2048,1536]{1,0:T(8,128)(2,1)}) %all-gather.15.cloned.1.call-update) | async-done | bytes 6291472 | tf_op jit(solution)/shard_map/all_gather | solution.py:192
  650.9 99.5 %all-gather.17.cloned.1.call-done = bf16[1536,2048]{1,0:T(8,128)(2,1)} async-done(((bf16[1536,256]{1,0:T(8,128)(2,1)}), bf16[1536,2048]{1,0:T(8,128)(2,1)}) %all-gather.17.cloned.1.call-update) | async-done | bytes 6291472 | tf_op jit(solution)/shard_map/all_gather | solution.py:198
  750.4 21.0 %convolution_convert_fusion = bf16[1024,2048]{1,0:T(8,128)(2,1)} fusion(bf16[1536,2048]{1,0:T(8,128)(2,1)} %all-gather.17.cloned.1.call-done, f32[1024,1536]{1,0:T(8,128)} %fusion.91, bf16[1024,2048]{1,0:T(8,128)(2,1)} %all-gather.11.cloned.1.call-done, bf16[2048,1536]{1,0:T(8,128)(2,1)} %all-gather.15.cloned.1.call-done), kind=kOutput, calls=%fused_computation.60 | convolution fusion | flops 12896436224 | bytes 27262976 | tf_op jit(solution)/shard_map/dot_general | solution.py:196
  771.4 42.9 %reduce-scatter.5.cloned.1.call-done = bf16[256,2048]{1,0:T(8,128)(2,1)} async-done(((bf16[1024,2048]{1,0:T(8,128)(2,1)}), bf16[256,2048]{1,0:T(8,128)(2,1)}) %reduce-scatter.5.cloned.1.call-update) | async-done | bytes 1048592 | tf_op jit(solution)/shard_map/reduce_scatter | solution.py:201
  814.3 2.8 fusion.36
  (505 shorter events, 284.0 us)
Async XLA Ops:
  7.4 26.6 %copy-start.12 = (f32[1024]{0:T(1024)S(1)}, f32[1024]{0:T(1024)}, u32[]{:S(2)}) copy-start(f32[1024]{0:T(1024)} %param.29) | copy-start | bytes 12292
  7.4 26.6 %copy-start.9 = (bf16[1024,128]{1,0:T(8,128)(2,1)S(1)}, bf16[1024,128]{1,0:T(8,128)(2,1)}, u32[]{:S(2)}) copy-start(bf16[1024,128]{1,0:T(8,128)(2,1)} %param.28) | copy-start | bytes 786436
  7.4 452.5 %reduce-scatter.3.cloned.1.call-start = ((), (), s32[]{:S(2)}) async-start(), calls=%async_computation.2 | async-start | bytes 5242880 | tf_op jit(solution)/shard_map/reduce_scatter | solution.py:174
  35.9 23.7 %copy-start.8 = (bf16[1024,256]{1,0:T(8,128)(2,1)S(1)}, bf16[1024,256]{1,0:T(8,128)(2,1)}, u32[]{:S(2)}) copy-start(bf16[1024,256]{1,0:T(8,128)(2,1)} %param.23) | copy-start | bytes 1572868
  37.2 22.4 %copy-start.2 = (f32[16,2,64,64]{3,0,1,2:T(8,128)}, f32[16,2,64,64]{3,0,1,2:T(8,128)S(1)}, u32[]{:S(2)}) copy-start(f32[16,2,64,64]{3,0,1,2:T(8,128)S(1)} %fusion.55) | copy-start | bytes 1572868
  67.2 135.2 %copy-start.10 = (bf16[1024,128]{1,0:T(8,128)(2,1)S(1)}, bf16[1024,128]{1,0:T(8,128)(2,1)}, u32[]{:S(2)}) copy-start(bf16[1024,128]{1,0:T(8,128)(2,1)} %param.25) | copy-start | bytes 786436
  166.1 40.3 %copy-start.11 = (bf16[1024,128]{1,0:T(8,128)(2,1)S(1)}, bf16[1024,128]{1,0:T(8,128)(2,1)}, u32[]{:S(2)}) copy-start(bf16[1024,128]{1,0:T(8,128)(2,1)} %param.26) | copy-start | bytes 786436
  384.6 8.2 copy-start.14
  388.9 5.8 copy-start.5
  409.7 2.9 copy-start.3
  409.7 2.9 copy-start.4
  409.7 2.9 copy-start.6
  409.7 3.0 copy-start.7
  416.2 43.6 %copy-start = (bf16[256,2048]{1,0:T(8,128)(2,1)S(1)}, bf16[256,2048]{1,0:T(8,128)(2,1)}, u32[]{:S(2)}) copy-start(bf16[256,2048]{1,0:T(8,128)(2,1)} %param.22) | copy-start | bytes 3145732
  416.2 45.6 %copy-start.13 = (f32[2048]{0:T(1024)S(1)}, f32[2048]{0:T(1024)}, u32[]{:S(2)}) copy-start(f32[2048]{0:T(1024)} %param.34) | copy-start | bytes 24580
  416.2 100.1 %all-gather.13.cloned.1.call-start = ((), (), s32[]{:S(2)}) async-start(), calls=%async_computation.4 | async-start | bytes 7077888 | tf_op jit(solution)/shard_map/all_gather | solution.py:187
  416.8 133.5 %all-gather.11.cloned.1.call-start = ((), (), s32[]{:S(2)}) async-start(), calls=%async_computation.3 | async-start | bytes 5242880 | tf_op jit(solution)/shard_map/all_gather | solution.py:184
  464.4 186.5 %all-gather.15.cloned.1.call-start = ((), (), s32[]{:S(2)}) async-start(), calls=%async_computation.5 | async-start | bytes 7077888 | tf_op jit(solution)/shard_map/all_gather | solution.py:192
  465.0 285.5 %all-gather.17.cloned.1.call-start = ((), (), s32[]{:S(2)}) async-start(), calls=%async_computation.6 | async-start | bytes 7077888 | tf_op jit(solution)/shard_map/all_gather | solution.py:198
  465.7 348.6 %reduce-scatter.5.cloned.1.call-start = ((), (), s32[]{:S(2)}) async-start(), calls=%async_computation.7 | async-start | bytes 5242880 | tf_op jit(solution)/shard_map/reduce_scatter | solution.py:201
  771.4 42.9 %copy-start.1 = (bf16[256,2048]{1,0:T(8,128)(2,1)S(1)}, bf16[256,2048]{1,0:T(8,128)(2,1)}, u32[]{:S(2)}) copy-start(bf16[256,2048]{1,0:T(8,128)(2,1)} %reduce-scatter.3.cloned.1.call-done) | copy-start | bytes 3145732
Sparse Core Ops, SparseCore 0:
  416.4 43.4 reduce-scatter.2
  771.5 42.7 reduce-scatter.4
Sparse Core Ops, SparseCore 1:
  418.9 97.4 all-gather.12
  517.8 32.5 all-gather.10
  552.4 98.5 all-gather.14
  653.0 97.4 all-gather.16
where the time goes:
time: 830 us; the launch traced here: 825 us
  waiting for transfers between devices  361 us (43%)
  other arithmetic  134 us (16%)
  local copies, waits for them, and re-layouts  104 us (13%)
  blocking collectives  104 us (13%)
  matrix products  103 us (12%)
  between operations  15.3 us (2%)
    all_gather x4, blocking collectives, entering(): lax.all_gather(part.astype(kind), axis)  104 us
    all_gather x1, waiting for transfers between devices, per_device(): lax.all_gather(down_projection, 'sp', axis=1, tiled=True)  99.5 us
    all_gather x1, waiting for transfers between devices, per_device(): lax.all_gather(up_projection, 'sp', axis=0, tiled=True)  88.9 us
    reduce_sum x32, other arithmetic, advance(): jnp.sum(query_piece[:, :, None, :] * key_piece[:, None, :, :] * decay_gri...  63.8 us
    all_gather x1, waiting for transfers between devices, per_device(): lax.all_gather(gate_projection, 'sp', axis=0, tiled=True)  50.6 us
    dynamic_slice x80, local copies, waits for them, and re-layouts, within_block_pass(): lax.scan(advance, zero_state, (query_blocks, key_blocks, value_blocks, de...  49.8 us
    reduce_scatter x1, waiting for transfers between devices, per_device(): lax.psum_scatter((jnp.dot(gated_a, output_projection[0], preferred_elemen...  43 us
    reduce_scatter x1, waiting for transfers between devices, per_device(): lax.psum_scatter(down_terms.astype(jnp.bfloat16), 'tp', scatter_dimension...  42.9 us
  transfers between devices with their start and end apart: 6, of which 6 were waited for; matrix products, arithmetic and copies ran while one was open for 2% of the time, Pallas kernels for 0%

commit v1 on v0

v1 whole, which is shorter than its diff:
```python
import jax
import jax.numpy as jnp
from jax import lax
from jax.experimental import pallas as pl
from jax.experimental.pallas import tpu as pltpu
from jax.sharding import PartitionSpec as P

FIRST_KEY_SIZE = 128
SECOND_KEY_SIZE = 64
DV = 128
CHUNK = 128
MIDDLE = CHUNK // 2 - 1
PAD = 16

EPS = 1e-06
SOFTNESS_SCALE = 16.0


def dot(a, b, dims):
    return lax.dot_general(a, b, (dims, ((), ())), preferred_element_type=jnp.float32)


def positions():
    row = lax.broadcasted_iota(jnp.int32, (CHUNK, CHUNK), 0)
    column = lax.broadcasted_iota(jnp.int32, (CHUNK, CHUNK), 1)
    return row, column


def fading_sums(fading_row):
    row, column = positions()
    as_column = jnp.sum(jnp.where(row == column, fading_row, 0.0), axis=1, keepdims=True)
    column_sums = jnp.sum(jnp.where(column <= row, fading_row, 0.0), axis=1, keepdims=True)
    row_sums = jnp.sum(jnp.where(row <= column, as_column, 0.0), axis=0, keepdims=True)
    return column_sums, row_sums


def channel_sums(switches):
    row, column = positions()
    x = switches.astype(jnp.float32)
    logs = (jnp.minimum(x, 0.0) - jnp.log1p(jnp.exp(-jnp.abs(x)))) * (1.0 / SOFTNESS_SCALE)
    lower = (column <= row).astype(jnp.bfloat16)
    high = logs.astype(jnp.bfloat16)
    low = (logs - high.astype(jnp.float32)).astype(jnp.bfloat16)
    return dot(lower, high, ((1,), (0,))) + dot(lower, low, ((1,), (0,)))


def lanes_of(head, width, key_width):
    lane = lax.broadcasted_iota(jnp.int32, (1, width), 1)
    return (lane >= head * key_width) & (lane < (head + 1) * key_width)


def advanced(state, inverse_keys, weighted, sums, total_fading, key_width):
    width = state.shape[1]
    end, middle = sums[CHUNK - 1 :, :], sums[MIDDLE : MIDDLE + 1, :]
    head_count = width // key_width
    if key_width % 128 == 0:
        added = jnp.concatenate(
            [
                dot(
                    weighted[:, h * DV : (h + 1) * DV],
                    inverse_keys[:, h * key_width : (h + 1) * key_width],
                    ((0,), (0,)),
                )
                for h in range(head_count)
            ],
            axis=1,
        )
    else:
        added = jnp.zeros((DV, width), jnp.float32)
        for h in range(head_count):
            product = dot(weighted[:, h * DV : (h + 1) * DV], inverse_keys, ((0,), (0,)))
            added = jnp.where(lanes_of(h, width, key_width), product, added)
    return jnp.exp(end + total_fading) * state + jnp.exp(end - middle) * added


def state_kernel(
    keys_a, keys_b, switches_a, switches_b, fading, values, packed, state_a, state_b, decay
):
    step = pl.program_id(0)
    width_a = keys_a.shape[1]

    @pl.when(step == 0)
    def _():
        state_a[...] = jnp.zeros_like(state_a)
        state_b[...] = jnp.zeros_like(state_b)
        decay[...] = jnp.zeros_like(decay)

    column_sums, _ = fading_sums(fading[0])
    total_fading = column_sums[CHUNK - 1 :, :]
    later = jnp.exp(total_fading - column_sums)
    for group, (keys, switches, state, key_width, start) in enumerate(
        (
            (keys_a, switches_a, state_a, FIRST_KEY_SIZE, 0),
            (keys_b, switches_b, state_b, SECOND_KEY_SIZE, width_a),
        )
    ):
        width = keys.shape[1]
        sums = channel_sums(switches[...])
        middle = sums[MIDDLE : MIDDLE + 1, :]
        inverse_keys = (keys[...].astype(jnp.float32) * jnp.exp(middle - sums)).astype(jnp.bfloat16)
        weighted = (values[group].astype(jnp.float32) * later).astype(jnp.bfloat16)
        state[...] = advanced(state[...], inverse_keys, weighted, sums, total_fading, key_width)
        decay[:, start : start + width] += sums[CHUNK - 1 :, :] + total_fading

    @pl.when(step == pl.num_programs(0) - 1)
    def _():
        packed[:DV, :width_a] = state_a[...].astype(jnp.bfloat16)
        packed[:DV, width_a:] = state_b[...].astype(jnp.bfloat16)
        packed[DV:, :] = jnp.broadcast_to(jnp.exp(decay[:1, :]), (PAD, decay.shape[1])).astype(
            jnp.bfloat16
        )


def output_kernel(
    place,
    everything,
    queries_a,
    queries_b,
    keys_a,
    keys_b,
    switches_a,
    switches_b,
    fading,
    values,
    gates,
    gains,
    projection,
    out,
    state_a,
    state_b,
):
    step = pl.program_id(0)
    width_a = keys_a.shape[1]

    @pl.when(step == 0)
    def _():
        state_a[...] = jnp.zeros_like(state_a)
        state_b[...] = jnp.zeros_like(state_b)

        @pl.loop(0, place[0])
        def _(k):
            part = everything[k].astype(jnp.float32)
            factor = part[DV : DV + 1, :]
            state_a[...] = factor[:, :width_a] * state_a[...] + part[:DV, :width_a]
            state_b[...] = factor[:, width_a:] * state_b[...] + part[:DV, width_a:]

    row, column = positions()
    causal = column <= row
    column_sums, row_sums = fading_sums(fading[0])
    total_fading = column_sums[CHUNK - 1 :, :]
    later = jnp.exp(total_fading - column_sums)
    since_start = jnp.exp(column_sums)
    between = jnp.exp(jnp.minimum(column_sums - row_sums, 0.0))
    summed = jnp.zeros(out.shape, jnp.float32)
    for group, (queries, keys, switches, state, key_width) in enumerate(
        (
            (queries_a, keys_a, switches_a, state_a, FIRST_KEY_SIZE),
            (queries_b, keys_b, switches_b, state_b, SECOND_KEY_SIZE),
        )
    ):
        width = keys.shape[1]
        sums = channel_sums(switches[...])
        middle = sums[MIDDLE : MIDDLE + 1, :]
        scaled = queries[...].astype(jnp.float32) * (jnp.exp(sums - middle) * key_width**-0.5)
        scaled = scaled.astype(jnp.bfloat16)
        inverse_keys = (keys[...].astype(jnp.float32) * jnp.exp(middle - sums)).astype(jnp.bfloat16)
        before = (state[...] * jnp.exp(middle)).astype(jnp.bfloat16)
        pieces = []
        for h in range(width // key_width):
            here = slice(h * DV, (h + 1) * DV)
            if key_width % 128 == 0:
                mine = slice(h * key_width, (h + 1) * key_width)
                q, k, s = scaled[:, mine], inverse_keys[:, mine], before[:, mine]
            else:
                q = jnp.where(lanes_of(h, width, key_width), scaled, jnp.zeros_like(scaled))
                k, s = inverse_keys, before
            scores = dot(q, k, ((1,), (1,))) * between
            scores = jnp.where(causal, scores, 0.0).astype(jnp.bfloat16)
            head = dot(scores, values[group, :, here], ((1,), (0,)))
            head = head + since_start * dot(q, s, ((1,), (1,)))
            inverse = lax.rsqrt(jnp.mean(head * head, axis=-1, keepdims=True) + EPS)
            gate = gates[group, :, here].astype(jnp.float32)
            silu = gate / (1.0 + jnp.exp(-gate))
            pieces.append((silu * (head * inverse * gains[group : group + 1, here])).astype(jnp.bfloat16))
        gated = pieces[0] if len(pieces) == 1 else jnp.concatenate(pieces, axis=1)
        summed = summed + dot(gated, projection[group], ((1,), (0,)))
        weighted = (values[group].astype(jnp.float32) * later).astype(jnp.bfloat16)
        state[...] = advanced(state[...], inverse_keys, weighted, sums, total_fading, key_width)
    out[...] = summed.astype(out.dtype)


def rows_of(array):
    return pl.BlockSpec((CHUNK, array.shape[1]), lambda i: (i, 0))


def pair_rows_of(array):
    return pl.BlockSpec((2, CHUNK, array.shape[2]), lambda i: (0, i, 0))


def whole(array):
    return pl.BlockSpec(array.shape, lambda i: (0,) * array.ndim)


def attention_terms(qa, ka, qb, kb, sa, sb, fading, values, gates, gains, projection):
    rows = qa.shape[0]
    steps = rows // CHUNK
    width_a, width_b = ka.shape[1], kb.shape[1]
    lines = fading.reshape(steps, 1, CHUNK)
    line_spec = pl.BlockSpec((1, 1, CHUNK), lambda i: (i, 0, 0))
    states = [pltpu.VMEM((DV, width_a), jnp.float32), pltpu.VMEM((DV, width_b), jnp.float32)]
    params = pltpu.CompilerParams(dimension_semantics=("arbitrary",))
    packed = pl.pallas_call(
        state_kernel,
        grid=(steps,),
        in_specs=[rows_of(ka), rows_of(kb), rows_of(sa), rows_of(sb), line_spec, pair_rows_of(values)],
        out_specs=pl.BlockSpec((DV + PAD, width_a + width_b), lambda i: (0, 0)),
        out_shape=jax.ShapeDtypeStruct((DV + PAD, width_a + width_b), jnp.bfloat16),
        scratch_shapes=states + [pltpu.VMEM((8, width_a + width_b), jnp.float32)],
        compiler_params=params,
        cost_estimate=pl.CostEstimate(flops=4_000_000_000, bytes_accessed=8_000_000, transcendentals=0),
        name="states",
    )(ka, kb, sa, sb, lines, values)
    everything = lax.all_gather(packed, "sp")
    place = lax.axis_index("sp").astype(jnp.int32).reshape(1)
    return pl.pallas_call(
        output_kernel,
        grid=(steps,),
        in_specs=[
            pl.BlockSpec(memory_space=pltpu.SMEM),
            whole(everything),
            rows_of(qa),
            rows_of(qb),
            rows_of(ka),
            rows_of(kb),
            rows_of(sa),
            rows_of(sb),
            line_spec,
            pair_rows_of(values),
            pair_rows_of(gates),
            whole(gains),
            whole(projection),
        ],
        out_specs=pl.BlockSpec((CHUNK, projection.shape[2]), lambda i: (i, 0)),
        out_shape=jax.ShapeDtypeStruct((rows, projection.shape[2]), jnp.bfloat16),
        scratch_shapes=states,
        compiler_params=params,
        cost_estimate=pl.CostEstimate(flops=8_000_000_000, bytes_accessed=16_000_000, transcendentals=0),
        name="outputs",
    )(place, everything, qa, qb, ka, kb, sa, sb, lines, values, gates, gains, projection)


def row_norm(source, gain_row):
    widened = source.astype(jnp.float32)
    inverse = lax.rsqrt(jnp.mean(widened * widened, axis=-1, keepdims=True) + EPS)
    return (widened * inverse * gain_row).astype(jnp.bfloat16)


def per_device(
    residual,
    first_group_queries,
    first_group_keys,
    second_group_queries,
    second_group_keys,
    primary_retain_switch_inputs,
    secondary_retain_switch_inputs,
    timestep_fading_exponent,
    values,
    output_gate_logits,
    head_norm_gains,
    output_projection,
    feedforward_norm_gain,
    gate_projection,
    up_projection,
    down_projection,
):
    terms = attention_terms(
        first_group_queries,
        first_group_keys,
        second_group_queries,
        second_group_keys,
        primary_retain_switch_inputs,
        secondary_retain_switch_inputs,
        timestep_fading_exponent,
        values,
        output_gate_logits,
        head_norm_gains,
        output_projection,
    )
    attention = lax.psum_scatter(terms, "tp", scatter_dimension=0, tiled=True).astype(jnp.float32)
    mid_rows = (residual.astype(jnp.float32) + attention).astype(jnp.bfloat16)
    all_rows = lax.all_gather(row_norm(mid_rows, feedforward_norm_gain), "tp", axis=0, tiled=True)
    gate_sum = jnp.dot(
        all_rows,
        lax.all_gather(gate_projection, "sp", axis=0, tiled=True),
        preferred_element_type=jnp.float32,
    )
    up_sum = jnp.dot(
        all_rows,
        lax.all_gather(up_projection, "sp", axis=0, tiled=True),
        preferred_element_type=jnp.float32,
    )
    hidden = (jax.nn.silu(gate_sum) * up_sum).astype(jnp.bfloat16)
    down_terms = jnp.dot(
        hidden,
        lax.all_gather(down_projection, "sp", axis=1, tiled=True),
        preferred_element_type=jnp.float32,
    )
    down_sum = lax.psum_scatter(
        down_terms.astype(jnp.bfloat16), "tp", scatter_dimension=0, tiled=True
    ).astype(jnp.float32)
    return (mid_rows.astype(jnp.float32) + down_sum).astype(jnp.bfloat16)


def solution(mesh):
    return jax.shard_map(
        per_device,
        mesh=mesh,
        in_specs=(
            P(("sp", "tp"), None),
            P("sp", "tp"),
            P("sp", "tp"),
            P("sp", "tp"),
            P("sp", "tp"),
            P("sp", "tp"),
            P("sp", "tp"),
            P("sp"),
            P(None, "sp", "tp"),
            P(None, "sp", "tp"),
            P(None, "tp"),
            P(None, "tp", None),
            P(),
            P("sp", "tp"),
            P("sp", "tp"),
            P("tp", "sp"),
        ),
        out_specs=P(("sp", "tp"), None),
        check_vma=False,
    )
```

time: 830 us -> 480 us (0.58)
  other arithmetic: 134 us -> 7.23 us
  local copies, waits for them, and re-layouts: 104 us -> 0.01 us
  matrix products: 103 us -> 32.7 us
  blocking collectives: 104 us -> 36.4 us
  Pallas kernels: 0 us -> 24.7 us
    dot_general x100 -> x0, matrix products: 70.7 us -> none  [the longest x32 40.8 us: advance(): jnp.einsum('rus,rsp->rup', query_piece * jnp.exp(decay_piece), running_st...]
    all_gather x4 -> x1, blocking collectives: 104 us -> 36.4 us  [attention_terms(): everything = lax.all_gather(packed, 'sp')]
    reduce_sum x33 -> x0, other arithmetic: 64.4 us -> none  [the longest x32 63.8 us: advance(): jnp.sum(query_piece[:, :, None, :] * key_piece[:, None, :, :] * decay_gri...]
    dynamic_slice x80 -> x0, local copies, waits for them, and re-layouts: 49.8 us -> none  [within_block_pass(): lax.scan(advance, zero_state, (query_blocks, key_blocks, value_blocks, de...]
    select_n x16 -> x0, other arithmetic: 24.7 us -> none  [step(): return jax.tree.map(lambda a, b: jnp.where(reached, a, b), new, before)]
    pallas_call x0 -> x2, Pallas kernels: none -> 24.7 us  [the longest x1 16.6 us: attention_terms(): pl.pallas_call(output_kernel, grid=(steps,), in_specs=[pl.BlockSpec(memor...]
    mul x20 -> x0, other arithmetic: 20.2 us -> none  [the longest x16 15.1 us: advance(): key_piece * jnp.exp(final_log_decay - decay_piece)]
    mul x24 -> x0, local copies, waits for them, and re-layouts: 16.3 us -> none  [the longest x4 10.1 us: finish(): normed = (summed * inverse).reshape(row_count, -1) * gain_row]
  transfers between devices with their start and end apart: 6 -> 6, of which waited for: 6 -> 6; matrix products, arithmetic and copies ran while one was open for 2% -> 3% of each run, Pallas kernels for 0% -> 0%
where the time goes in v1:
time: 480 us; the launch traced here: 479 us
  waiting for transfers between devices  363 us (76%)
  blocking collectives  36.4 us (8%)
  matrix products  32.7 us (7%)
  Pallas kernels  24.7 us (5%)
  between operations  15.1 us (3%)
  other arithmetic  7.23 us (2%)
    all_gather x1, waiting for transfers between devices, per_device(): lax.all_gather(down_projection, 'sp', axis=1, tiled=True)  99.5 us
    all_gather x1, waiting for transfers between devices, per_device(): lax.all_gather(up_projection, 'sp', axis=0, tiled=True)  88.9 us
    all_gather x1, waiting for transfers between devices, per_device(): lax.all_gather(gate_projection, 'sp', axis=0, tiled=True)  50.6 us
    reduce_scatter x1, waiting for transfers between devices, per_device(): lax.psum_scatter(terms, 'tp', scatter_dimension=0, tiled=True)  45.2 us
    reduce_scatter x1, waiting for transfers between devices, per_device(): lax.psum_scatter(down_terms.astype(jnp.bfloat16), 'tp', scatter_dimension...  42.9 us
    all_gather x1, blocking collectives, attention_terms(): everything = lax.all_gather(packed, 'sp')  36.4 us
    all_gather x1, waiting for transfers between devices, per_device(): lax.all_gather(row_norm(mid_rows, feedforward_norm_gain), 'tp', axis=0, t...  34 us
    dot_general x1, matrix products, per_device(): jnp.dot(hidden, lax.all_gather(down_projection, 'sp', axis=1, tiled=True)...  21 us
  transfers between devices with their start and end apart: 6, of which 6 were waited for; matrix products, arithmetic and copies ran while one was open for 3% of the time, Pallas kernels for 0%

profile of v1, /device:TPU:0, one launch (start us, length us, event | category | flops | bytes accessed | tf_op | source)
XLA Modules:
  0.0 479.2 jit_solution(7925208736944446755)
XLA Ops:
  7.4 8.1 %states.1 = bf16[144,384]{1,0:T(8,128)(2,1)} custom-call(bf16[1024,256]{1,0:T(8,128)(2,1)} %keys_a.3, bf16[1024,128]{1,0:T(8,128)(2,1)} %keys_b.3, bf16[1024,256]{1,0:T(8,128)(2,1)} %switches_a.3, bf16[1024,128]{1,0:T(8,128)(2,1)} %switches_b.3, f32[8,1,128]{2,1,0:T(1,128)} %bitcast.18, bf16[2,1024,256]{2,1,0:T(8,128)(2,1)} %values.3), custom_call_target="tpu_custom_call" | custom-call | flops 4000000000 | bytes 8000000 | tf_op jit(solution)/shard_map/states/pallas_call | solution.py:212
  15.5 36.4 %all-gather = bf16[1152,384]{1,0:T(8,128)(2,1)} all-gather(bf16[144,384]{1,0:T(8,128)(2,1)} %states.1), channel_id=2, replica_groups=mesh['sp'=8,'tp'=4] {'sp'}, dimensions={0}, use_global_device_ids=true | all-gather | bytes 995328 | tf_op jit(solution)/shard_map/all_gather | solution.py:223
  51.9 16.6 %outputs.1 = bf16[1024,2048]{1,0:T(8,128)(2,1)} custom-call(s32[1]{0:T(128)} %bitcast.place, bf16[8,144,384]{2,1,0:T(8,128)(2,1)} %bitcast.17, bf16[1024,256]{1,0:T(8,128)(2,1)} %queries_a.1, bf16[1024,128]{1,0:T(8,128)(2,1)} %queries_b.1, bf16[1024,256]{1,0:T(8,128)(2,1)} %keys_a.3, bf16[1024,128]{1,0:T(8,128)(2,1)} %keys_b.3, ...), custom_call_target="tpu_custom_call" | custom-call | flops 8000000000 | bytes 16000000 | tf_op jit(solution)/shard_map/outputs/pallas_call | solution.py:225
  68.5 0.0 reduce-scatter.3.cloned.1.call-update
  68.6 0.0 all-gather.8.cloned.1.call-start
  68.6 0.5 all-gather.8.cloned.1.call-update
  69.1 0.0 all-gather.6.cloned.1.call-start
  69.2 45.2 %reduce-scatter.3.cloned.1.call-done = bf16[256,2048]{1,0:T(8,128)(2,1)} async-done(((bf16[1024,2048]{1,0:T(8,128)(2,1)}), bf16[256,2048]{1,0:T(8,128)(2,1)}) %reduce-scatter.3.cloned.1.call-update) | async-done | bytes 1048592 | tf_op jit(solution)/shard_map/reduce_scatter | solution.py:289
  114.4 1.9 fusion
  116.3 2.6 fusion.2
  118.9 0.0 all-gather.6.cloned.1.call-update
  119.0 0.0 all-gather.10.cloned.1.call-start
  119.0 0.5 all-gather.10.cloned.1.call-update
  119.5 0.0 all-gather.12.cloned.1.call-start
  119.6 0.7 all-gather.12.cloned.1.call-update
  120.3 0.0 reduce-scatter.5.cloned.1.call-start
  120.3 50.6 %all-gather.8.cloned.1.call-done = bf16[2048,1536]{1,0:T(8,128)(2,1)} async-done(((bf16[256,1536]{1,0:T(8,128)(2,1)}), bf16[2048,1536]{1,0:T(8,128)(2,1)}) %all-gather.8.cloned.1.call-update) | async-done | bytes 6291472 | tf_op jit(solution)/shard_map/all_gather | solution.py:294
  170.9 34.0 %all-gather.6.cloned.1.call-done = bf16[1024,2048]{1,0:T(8,128)(2,1)} async-done(((bf16[256,2048]{1,0:T(8,128)(2,1)}), bf16[1024,2048]{1,0:T(8,128)(2,1)}) %all-gather.6.cloned.1.call-update) | async-done | bytes 4194320 | tf_op jit(solution)/shard_map/all_gather | solution.py:291
  204.9 11.7 %fusion.4 = f32[1024,1536]{1,0:T(8,128)} fusion(bf16[1024,2048]{1,0:T(8,128)(2,1)} %all-gather.6.cloned.1.call-done, bf16[2048,1536]{1,0:T(8,128)(2,1)} %all-gather.8.cloned.1.call-done), kind=kOutput, calls=%fused_computation.11 | convolution fusion | flops 6442450944 | bytes 16777216 | tf_op jit(solution)/shard_map/dot_general | solution.py:292
  216.6 88.9 %all-gather.10.cloned.1.call-done = bf16[2048,1536]{1,0:T(8,128)(2,1)} async-done(((bf16[256,1536]{1,0:T(8,128)(2,1)}), bf16[2048,1536]{1,0:T(8,128)(2,1)}) %all-gather.10.cloned.1.call-update) | async-done | bytes 6291472 | tf_op jit(solution)/shard_map/all_gather | solution.py:299
  305.5 99.5 %all-gather.12.cloned.1.call-done = bf16[1536,2048]{1,0:T(8,128)(2,1)} async-done(((bf16[1536,256]{1,0:T(8,128)(2,1)}), bf16[1536,2048]{1,0:T(8,128)(2,1)}) %all-gather.12.cloned.1.call-update) | async-done | bytes 6291472 | tf_op jit(solution)/shard_map/all_gather | solution.py:305
  405.0 21.0 %convolution_convert_fusion = bf16[1024,2048]{1,0:T(8,128)(2,1)} fusion(bf16[1536,2048]{1,0:T(8,128)(2,1)} %all-gather.12.cloned.1.call-done, f32[1024,1536]{1,0:T(8,128)} %fusion.4, bf16[1024,2048]{1,0:T(8,128)(2,1)} %all-gather.6.cloned.1.call-done, bf16[2048,1536]{1,0:T(8,128)(2,1)} %all-gather.10.cloned.1.call-done), kind=kOutput, calls=%fused_computation.1 | convolution fusion | flops 12896436224 | bytes 27262976 | tf_op jit(solution)/shard_map/dot_general | solution.py:303
  426.0 42.9 %reduce-scatter.5.cloned.1.call-done = bf16[256,2048]{1,0:T(8,128)(2,1)} async-done(((bf16[1024,2048]{1,0:T(8,128)(2,1)}), bf16[256,2048]{1,0:T(8,128)(2,1)}) %reduce-scatter.5.cloned.1.call-update) | async-done | bytes 1048592 | tf_op jit(solution)/shard_map/reduce_scatter | solution.py:308
  468.9 2.7 fusion.3
  (9 shorter events, 0.0 us)
Async XLA Ops:
  7.4 107.1 %reduce-scatter.3.cloned.1.call-start = ((), (), s32[]{:S(2)}) async-start(), calls=%async_computation.2 | async-start | bytes 5242880 | tf_op jit(solution)/shard_map/reduce_scatter | solution.py:289
  68.5 45.9 %copy-start = (bf16[256,2048]{1,0:T(8,128)(2,1)S(1)}, bf16[256,2048]{1,0:T(8,128)(2,1)}, u32[]{:S(2)}) copy-start(bf16[256,2048]{1,0:T(8,128)(2,1)} %param.16) | copy-start | bytes 3145732
  68.5 47.8 %copy-start.2 = (f32[2048]{0:T(1024)S(1)}, f32[2048]{0:T(1024)}, u32[]{:S(2)}) copy-start(f32[2048]{0:T(1024)} %param.28) | copy-start | bytes 24580
  68.6 102.4 %all-gather.8.cloned.1.call-start = ((), (), s32[]{:S(2)}) async-start(), calls=%async_computation.4 | async-start | bytes 7077888 | tf_op jit(solution)/shard_map/all_gather | solution.py:294
  69.1 135.7 %all-gather.6.cloned.1.call-start = ((), (), s32[]{:S(2)}) async-start(), calls=%async_computation.3 | async-start | bytes 5242880 | tf_op jit(solution)/shard_map/all_gather | solution.py:291
  119.0 186.5 %all-gather.10.cloned.1.call-start = ((), (), s32[]{:S(2)}) async-start(), calls=%async_computation.5 | async-start | bytes 7077888 | tf_op jit(solution)/shard_map/all_gather | solution.py:299
  119.5 285.4 %all-gather.12.cloned.1.call-start = ((), (), s32[]{:S(2)}) async-start(), calls=%async_computation.6 | async-start | bytes 7077888 | tf_op jit(solution)/shard_map/all_gather | solution.py:305
  120.3 348.6 %reduce-scatter.5.cloned.1.call-start = ((), (), s32[]{:S(2)}) async-start(), calls=%async_computation.7 | async-start | bytes 5242880 | tf_op jit(solution)/shard_map/reduce_scatter | solution.py:308
  425.9 43.0 %copy-start.1 = (bf16[256,2048]{1,0:T(8,128)(2,1)S(1)}, bf16[256,2048]{1,0:T(8,128)(2,1)}, u32[]{:S(2)}) copy-start(bf16[256,2048]{1,0:T(8,128)(2,1)} %reduce-scatter.3.cloned.1.call-done) | copy-start | bytes 3145732
Sparse Core Ops, SparseCore 0:
  68.7 45.7 reduce-scatter.2
  426.1 42.7 reduce-scatter.4
Sparse Core Ops, SparseCore 1:
  71.2 99.6 all-gather.7
  172.3 32.5 all-gather.5
  206.9 98.5 all-gather.9
  307.5 97.4 all-gather.11
